TPU v7x, 512 devices: a whole 4x8x8 slice. The times are simulated.
512 devices in a mesh: dp: 4 (over x), kv: 64 (over z, y), tp: 2 (over core).
Axes of the slice: x: 4, y: 8, z: 8, core: 2. Of those that a mesh axis runs over, the one named last changes fastest.
Arguments:
- tokens: bfloat16 [16, 4096], P('dp', ('kv', 'tp')), may hold values from -11 to 11
- attn_gain: float32 [4096], replicated, may hold values from 0.1 to 1.9
- query_weight: bfloat16 [4096, 4096], P('kv', 'tp'), may hold values from -0.09375 to 0.09375
- key_cache: bfloat16 [16, 16384, 2, 128], P('dp', 'kv', 'tp'), may hold values from -820 to 820
- value_cache: bfloat16 [16, 16384, 2, 128], P('dp', 'kv', 'tp'), may hold values from -6 to 6
- head_lambda: float32 [32], P('tp'), may hold values from 0.3 to 0.8
- head_gain: float32 [128], replicated, may hold values from 0.1 to 1.9
- out_weight: bfloat16 [4096, 4096], P('kv', 'tp'), may hold values from -0.09375 to 0.09375
- mlp_gain: float32 [4096], replicated, may hold values from 0.1 to 1.9
- gate_weight: bfloat16 [11264, 4096], P(('kv', 'tp')), may hold values from -0.09375 to 0.09375
- up_weight: bfloat16 [11264, 4096], P(('kv', 'tp')), may hold values from -0.09375 to 0.09375
- down_weight: bfloat16 [11264, 4096], P(('kv', 'tp')), may hold values from -0.21875 to 0.21875
Outputs:
- mixed: bfloat16 [16, 4096], P('dp', ('kv', 'tp'))
All inputs are finite; a program needn't handle non-finite values.
Results may differ from a plain program's by a relative error of at most 0.02.
The roundings to bfloat16 on the way count: a program that leaves them out, or rounds other values in their place, can miss the bound.
Values may be sent and summed in bfloat16 or wider, within the bound.
No kernel may reach another device: no remote copies, remote signals or barrier semaphores. Data moves between devices by JAX's collectives and lax.ppermute only.
A program may use at most 64 MiB of HBM per device.

v0:
```python
import jax
import jax.numpy as jnp
from jax import lax
from jax.sharding import Mesh
from jax.sharding import PartitionSpec as P

KV = ("kv_0", "kv_1")
KV_TP = ("kv_0", "kv_1", "tp")
EPS = 1e-06
THETA = 10000.0


def sent_to_all(x, axis):
    copies = jnp.broadcast_to(x, (lax.axis_size(axis), *x.shape))
    return lax.all_to_all(copies, axis, split_axis=0, concat_axis=0, tiled=True)


def joined_along(pieces, dim):
    shape = list(pieces.shape[1:])
    shape[dim] *= pieces.shape[0]
    return jnp.moveaxis(pieces, 0, dim).reshape(shape)


def whole_of(x, axes, dim):
    far, near = axes
    first = sent_to_all(x, far)
    pieces = jnp.swapaxes(sent_to_all(first, near), 0, 1)
    return joined_along(pieces.reshape(-1, *x.shape), dim)


def one_axis_at_a_time(x, axes):
    for axis in axes:
        x = lax.psum(x, axis)
    return x


def collected_together(x, axis):
    leaves = jax.tree.leaves(x)
    turns = sorted(range(len(leaves)), key=lambda k: -leaves[k].size)
    width = (1, *leaves[turns[0]].shape)[-1]
    lines = [
        jnp.pad(leaves[k].reshape(-1), (0, -leaves[k].size % width)).reshape(-1, width)
        for k in turns
    ]
    both, at, found = (lax.all_gather(jnp.concatenate(lines), axis), 0, {})
    for k, line in zip(turns, lines):
        slab = both[:, at : at + len(line)].reshape(len(both), -1)
        found[k] = slab[:, : leaves[k].size].reshape(-1, *leaves[k].shape)
        at += len(line)
    numbers = iter(range(len(leaves)))
    return jax.tree.map(lambda _: found[next(numbers)], x)


def merged_by_axis(x, axes, combine):
    for axis in axes:
        pieces = collected_together(x, axis)
        x = jax.tree.map(lambda part: part[0], pieces)
        for k in range(1, lax.axis_size(axis)):
            x = combine(x, jax.tree.map(lambda part: part[k], pieces))
    return x


def split_up(x, dim, count):
    shape = x.shape
    pieces = x.reshape(*shape[:dim], count, shape[dim] // count, *shape[dim + 1 :])
    return jnp.moveaxis(pieces, dim, 0)


def sum_at_owner(x, axis, dim):
    count = lax.axis_size(axis)
    pieces = lax.all_to_all(split_up(x, dim, count), axis, 0, 0, tiled=True)
    return jnp.sum(pieces, axis=0)


def sum_by_axis(x, axes, dim):
    far, near = axes
    own = sum_at_owner(split_up(x, dim, lax.axis_size(far)), near, dim + 1)
    return jnp.sum(lax.all_to_all(own, far, 0, 0, tiled=True), axis=0)


def rotate(vector, position):
    half_len = vector.shape[-1] // 2
    inv_freq = 1.0 / THETA ** (jnp.arange(half_len, dtype=jnp.float32) / half_len)
    angles = position * inv_freq
    cos_table = jnp.cos(angles)
    sin_table = jnp.sin(angles)
    first_half = vector[..., :half_len]
    second_half = vector[..., half_len:]
    return jnp.concatenate(
        [
            first_half * cos_table - second_half * sin_table,
            second_half * cos_table + first_half * sin_table,
        ],
        axis=-1,
    )


def combine(earlier, latter):
    peak_a, total_a, value_a = earlier
    peak_b, total_b, value_b = latter
    peak_new = jnp.maximum(peak_a, peak_b)
    factor_a = jnp.exp(peak_a - peak_new)
    factor_b = jnp.exp(peak_b - peak_new)
    return (
        peak_new,
        total_a * factor_a + total_b * factor_b,
        value_a * factor_a[..., None] + value_b * factor_b[..., None],
    )


def inner_last(left, right):
    return lax.dot_general(
        left, right, (((1,), (1,)), ((), ())), preferred_element_type=jnp.float32
    )


def shards(
    tokens,
    attn_gain,
    query_weight,
    key_cache,
    value_cache,
    head_lambda,
    head_gain,
    out_weight,
    mlp_gain,
    gate_weight,
    up_weight,
    down_weight,
):
    row_count = tokens.shape[0]
    kv_count = lax.axis_size(KV)
    tp_count = lax.axis_size("tp")
    kv_index = lax.axis_index(KV)
    row_span = query_weight.shape[0]
    full_rows = whole_of(tokens, (("kv_0", "kv_1"), "tp"), 1)
    wide_rows = full_rows.astype(jnp.float32)
    mean_square = jnp.mean(wide_rows * wide_rows, axis=-1, keepdims=True)
    scaled = (wide_rows * attn_gain).astype(jnp.bfloat16)
    local_cols = lax.dynamic_slice_in_dim(scaled, kv_index * row_span, row_span, 1)
    queries = one_axis_at_a_time(
        jnp.dot(local_cols, query_weight, preferred_element_type=jnp.float32), KV
    )
    queries = queries * lax.rsqrt(mean_square + EPS)
    head_count = head_lambda.shape[0]
    kv_local = key_cache.shape[2]
    group_size = head_count // kv_local
    position_count = key_cache.shape[1]
    half_dim = key_cache.shape[3] // 2
    value_dim = value_cache.shape[3]
    queries = queries.reshape(row_count, kv_local, group_size, 2, half_dim)
    rotated = rotate(queries, jnp.float32(position_count * kv_count)).astype(jnp.bfloat16)
    key_grid = key_cache.reshape(row_count, position_count, kv_local, 2, half_dim)
    scores = jnp.einsum(
        "bkgch,bpkch->bkgcp", rotated, key_grid, preferred_element_type=jnp.float32
    ) * half_dim ** (-0.5)
    local_peak = jnp.max(scores, axis=-1)
    weights_exp = jnp.exp(scores - local_peak[..., None])
    lam_grid = head_lambda.reshape(kv_local, group_size)[None, :, :, None]
    exp_total = jnp.sum(weights_exp, axis=-1)
    weighted = jnp.einsum(
        "bkgcp,bpkv->bkgcv",
        weights_exp.astype(jnp.bfloat16),
        value_cache,
        preferred_element_type=jnp.float32,
    )
    peak_all, total_all, weighted_all = merged_by_axis(
        (local_peak, exp_total, weighted), KV, combine
    )
    attended = weighted_all / total_all[..., None]
    difference = attended[:, :, :, 0] - lam_grid * attended[:, :, :, 1]
    head_norm = lax.rsqrt(jnp.mean(difference * difference, axis=-1, keepdims=True) + EPS)
    head_out = (difference * head_norm * head_gain).reshape(row_count, head_count * value_dim)
    head_out = head_out.astype(jnp.bfloat16)
    out_part = inner_last(head_out, out_weight).astype(jnp.bfloat16)
    pieces = whole_of(out_part, (("kv_0", "kv_1"), "tp"), 1)
    attention = jnp.sum(
        pieces.astype(jnp.float32).reshape(row_count, kv_count, tp_count, -1), axis=2
    )
    stream = wide_rows + attention.reshape(row_count, -1)
    stream_square = jnp.mean(stream * stream, axis=-1, keepdims=True)
    normed = (stream * lax.rsqrt(stream_square + EPS) * mlp_gain).astype(jnp.bfloat16)
    gate_out = inner_last(normed, gate_weight)
    up_out = inner_last(normed, up_weight)
    hidden = (jax.nn.silu(gate_out) * up_out).astype(jnp.bfloat16)
    own_cols = tokens.shape[1]
    down_cols = sum_by_axis(
        lax.dot_general(
            down_weight, hidden, (((0,), (1,)), ((), ())), preferred_element_type=jnp.float32
        ),
        (("kv_0", "kv_1"), "tp"),
        0,
    )
    column_index = lax.axis_index(KV_TP)
    own_stream = lax.dynamic_slice_in_dim(stream, column_index * own_cols, own_cols, 1)
    return (own_stream + down_cols.T).astype(jnp.bfloat16)


def solution(mesh):
    torus = Mesh(
        mesh.devices.reshape(mesh.shape["dp"], 8, 8, mesh.shape["tp"]), ("dp", "kv_0", "kv_1", "tp")
    )
    in_specs = (
        P("dp", KV_TP),
        P(),
        P(KV, "tp"),
        P("dp", KV, "tp", None),
        P("dp", KV, "tp", None),
        P("tp"),
        P(),
        P(KV, "tp"),
        P(),
        P(KV_TP, None),
        P(KV_TP, None),
        P(KV_TP, None),
    )
    out_specs = P("dp", KV_TP)
    return jax.shard_map(
        shards, mesh=torus, in_specs=in_specs, out_specs=out_specs, check_vma=False
    )
```

profile of v0, /device:TPU:6, one launch (start us, length us, event | category | flops | bytes accessed | tf_op | source)
XLA Modules:
  0.0 199.4 jit_solution(2808983307863396402)
XLA Ops:
  0.0 1.4 broadcast_in_dim.8
  1.4 16.7 %all-to-all-start = ((bf16[64,4,32]{2,1,0:T(4,128)(2,1)}), bf16[64,4,32]{2,1,0:T(4,128)(2,1)S(1)}, u32[]{:S(2)}, u32[]{:S(2)}) async-start(bf16[64,4,32]{2,1,0:T(4,128)(2,1)} %broadcast_in_dim.8), calls=%async_computation | async-start | bytes 131072 | tf_op jit(solution)/shard_map/all_to_all | solution.py:15
  18.3 1.1 copy.28
  19.4 0.8 dynamic-slice
  20.1 10.2 %all-to-all-done = bf16[64,4,32]{2,1,0:T(4,128)(2,1)S(1)} async-done(((bf16[64,4,32]{2,1,0:T(4,128)(2,1)}), bf16[64,4,32]{2,1,0:T(4,128)(2,1)S(1)}, u32[]{:S(2)}, u32[]{:S(2)}) %all-to-all-start) | async-done | bytes 16416 | tf_op jit(solution)/shard_map/all_to_all | solution.py:15
  30.6 3.7 %all_to_all.30 = bf16[2,2,4096]{2,1,0:T(2,128)(2,1)S(1)} all-to-all(bf16[2,2,4096]{2,1,0:T(2,128)(2,1)S(1)} %reshape.2089), channel_id=1, replica_groups=mesh['dp'=4,'kv_0'=8,'kv_1'=8,'tp'=2] {'tp'}, dimensions={0} | all-to-all | bytes 65536 | tf_op jit(solution)/shard_map/all_to_all | solution.py:15
  34.9 0.7 copy-done.4
  35.6 0.2 fusion.48
  35.8 27.5 %psum.14 = f32[4,2048]{1,0:T(4,128)S(1)} all-reduce(f32[4,2048]{1,0:T(4,128)S(1)} %fusion.48), channel_id=1, replica_groups=mesh['dp'=4,'kv_0'=8,'kv_1'=8,'tp'=2] {'kv_0'}, use_global_device_ids=true, to_apply=%region_0.0 | all-reduce | flops 8192 | bytes 65536 | tf_op jit(solution)/shard_map/psum | solution.py:33
  63.3 27.6 %psum.15 = f32[4,2048]{1,0:T(4,128)S(1)} all-reduce(f32[4,2048]{1,0:T(4,128)S(1)} %psum.14), channel_id=1, replica_groups=mesh['dp'=4,'kv_0'=8,'kv_1'=8,'tp'=2] {'kv_1'}, use_global_device_ids=true, to_apply=%region_1.0 | all-reduce | flops 8192 | bytes 65536 | tf_op jit(solution)/shard_map/psum | solution.py:33
  91.3 0.3 fusion.100
  92.3 0.2 fusion.2
  92.6 25.3 %all-gather.2 = f32[8,130,128]{2,1,0:T(8,128)S(1)} all-gather(f32[1,130,128]{2,1,0:T(8,128)S(1)} %maximum_bitcast_fusion), channel_id=2, replica_groups=mesh['dp'=4,'kv_0'=8,'kv_1'=8,'tp'=2] {'kv_0'}, dimensions={0}, use_global_device_ids=true | all-gather | bytes 599040 | tf_op jit(solution)/shard_map/all_gather | solution.py:45
  118.0 0.3 fusion.9
  118.3 25.3 %all-gather.3 = f32[8,130,128]{2,1,0:T(8,128)S(1)} all-gather(f32[1,130,128]{2,1,0:T(8,128)S(1)} %maximum_bitcast_fusion.1), channel_id=3, replica_groups=mesh['dp'=4,'kv_0'=8,'kv_1'=8,'tp'=2] {'kv_1'}, dimensions={0}, use_global_device_ids=true | all-gather | bytes 599040 | tf_op jit(solution)/shard_map/all_gather | solution.py:45
  146.1 1.2 add_divide_fusion
  147.7 0.6 copy-done.5
  148.6 19.0 %all_to_all.31 = bf16[64,2,128]{2,1,0:T(2,128)(2,1)S(1)} all-to-all(bf16[64,2,128]{2,1,0:T(2,128)(2,1)S(1)} %reshape.2091), channel_id=1, replica_groups=mesh['dp'=4,'kv_0'=8,'kv_1'=8,'tp'=2] {'kv_0','kv_1'}, dimensions={0} | all-to-all | bytes 65536 | tf_op jit(solution)/shard_map/all_to_all | solution.py:15
  167.9 3.8 %all_to_all.32 = bf16[2,2,8192]{2,1,0:T(2,128)(2,1)S(1)} all-to-all(bf16[2,2,8192]{2,1,0:T(2,128)(2,1)S(1)} %reshape.2093), channel_id=1, replica_groups=mesh['dp'=4,'kv_0'=8,'kv_1'=8,'tp'=2] {'tp'}, dimensions={0} | all-to-all | bytes 131072 | tf_op jit(solution)/shard_map/all_to_all | solution.py:15
  171.9 0.4 bitcast_reduce_fusion
  172.8 0.7 copy-done.1
  173.5 0.3 fusion.95
  173.8 0.7 convolution_bitcast_fusion
  174.5 0.3 reshape_reshape.2
  175.1 3.8 %all_to_all.33 = f32[2,1,8192]{2,1,0:T(1,128)S(1)} all-to-all(f32[2,1,8192]{2,1,0:T(1,128)S(1)} %reshape.2095), channel_id=1, replica_groups=mesh['dp'=4,'kv_0'=8,'kv_1'=8,'tp'=2] {'tp'}, dimensions={0} | all-to-all | bytes 131072 | tf_op jit(solution)/shard_map/all_to_all | solution.py:71
  178.9 0.5 broadcast.362
  179.4 0.8 reduce.224
  180.5 0.7 reshape.2097
  181.2 4.6 %all-to-all-start.5 = ((f32[64,1,128]{2,1,0:T(1,128)}), f32[64,1,128]{2,1,0:T(1,128)S(1)}, u32[]{:S(2)}, u32[]{:S(2)}) async-start(f32[64,1,128]{2,1,0:T(1,128)} %reshape.2097), calls=%async_computation.5 | async-start | bytes 65536 | tf_op jit(solution)/shard_map/all_to_all | solution.py:78
  185.9 12.0 %all-to-all-done.5 = f32[64,1,128]{2,1,0:T(1,128)S(1)} async-done(((f32[64,1,128]{2,1,0:T(1,128)}), f32[64,1,128]{2,1,0:T(1,128)S(1)}, u32[]{:S(2)}, u32[]{:S(2)}) %all-to-all-start.5) | async-done | bytes 32800 | tf_op jit(solution)/shard_map/all_to_all | solution.py:78
  197.9 0.7 reduce.225
  198.8 0.6 fusion.44
  (88 shorter events, 6.6 us)
Async XLA Ops:
  0.0 173.8 %copy-start = (bf16[88,4096]{1,0:T(8,128)(2,1)S(1)}, bf16[88,4096]{1,0:T(8,128)(2,1)}, u32[]{:S(2)}) copy-start(bf16[88,4096]{1,0:T(8,128)(2,1)} %param.23) | copy-start | bytes 2162692
  1.4 16.7 %copy-start.7 = (f32[16]{0:T(128)S(1)}, f32[16]{0:T(128)}, u32[]{:S(2)}) copy-start(f32[16]{0:T(128)} %param.17) | copy-start | bytes 196
  1.4 16.7 %copy-start.8 = (f32[128]{0:T(128)S(1)}, f32[128]{0:T(128)}, u32[]{:S(2)}) copy-start(f32[128]{0:T(128)} %param.18) | copy-start | bytes 1540
  1.4 29.0 %all-to-all-start = ((bf16[64,4,32]{2,1,0:T(4,128)(2,1)}), bf16[64,4,32]{2,1,0:T(4,128)(2,1)S(1)}, u32[]{:S(2)}, u32[]{:S(2)}) async-start(bf16[64,4,32]{2,1,0:T(4,128)(2,1)} %broadcast_in_dim.8), calls=%async_computation | async-start | bytes 131072 | tf_op jit(solution)/shard_map/all_to_all | solution.py:15
  34.6 1.0 copy-start.4
  91.3 1.0 copy-start.3
  147.3 1.0 copy-start.5
  172.4 1.1 copy-start.1
  172.5 1.0 copy-start.6
  172.6 1.2 copy-start.2
  181.2 16.7 %all-to-all-start.5 = ((f32[64,1,128]{2,1,0:T(1,128)}), f32[64,1,128]{2,1,0:T(1,128)S(1)}, u32[]{:S(2)}, u32[]{:S(2)}) async-start(f32[64,1,128]{2,1,0:T(1,128)} %reshape.2097), calls=%async_computation.5 | async-start | bytes 65536 | tf_op jit(solution)/shard_map/all_to_all | solution.py:78
where the time goes:
time: 200 us; the launch traced here: 199 us
  blocking collectives  136 us (68%)
  waiting for transfers between devices  22.2 us (11%)
  starting transfers between devices  21.3 us (11%)
  local copies, waits for them, and re-layouts  12 us (6%)
  other arithmetic  5.28 us (3%)
    psum x2, blocking collectives, one_axis_at_a_time(): x = lax.psum(x, axis)  55.2 us
    all_gather x2, blocking collectives, collected_together(): both, at, found = (lax.all_gather(jnp.concatenate(lines), axis), 0, {})  50.6 us
    all_to_all x3, blocking collectives, sent_to_all(): return lax.all_to_all(copies, axis, split_axis=0, concat_axis=0, tiled=True)  26.6 us
    all_to_all x1, starting transfers between devices, sent_to_all(): return lax.all_to_all(copies, axis, split_axis=0, concat_axis=0, tiled=True)  16.7 us
    all_to_all x1, waiting for transfers between devices, sum_by_axis(): return jnp.sum(lax.all_to_all(own, far, 0, 0, tiled=True), axis=0)  12 us
    all_to_all x1, waiting for transfers between devices, sent_to_all(): return lax.all_to_all(copies, axis, split_axis=0, concat_axis=0, tiled=True)  10.2 us
    unnamed x32, local copies, waits for them, and re-layouts  5 us
    all_to_all x1, starting transfers between devices, sum_by_axis(): return jnp.sum(lax.all_to_all(own, far, 0, 0, tiled=True), axis=0)  4.61 us
  transfers between devices with their start and end apart: 2, of which 2 were waited for; matrix products, arithmetic and copies ran while one was open for 1% of the time, Pallas kernels for 0%

commit v1 on v0

--- a/solution.py
+++ b/solution.py
@@ -30,7 +30,7 @@
 
 def one_axis_at_a_time(x, axes):
     for axis in axes:
-        x = lax.psum(x, axis)
+        x = jnp.sum(lax.all_gather(x, axis), axis=0)
     return x
 
 

time: 200 us -> 192 us (0.960)
  blocking collectives: 136 us -> 129 us
    psum x2 -> x0, blocking collectives: 55.2 us -> none  [one_axis_at_a_time(): x = lax.psum(x, axis)]
    all_gather x0 -> x2, blocking collectives: none -> 49.6 us  [one_axis_at_a_time(): x = jnp.sum(lax.all_gather(x, axis), axis=0)]
where the time goes in v1:
time: 192 us
  blocking collectives  129 us (67%)
  waiting for transfers between devices  22.2 us (12%)
  starting transfers between devices  21.3 us (11%)
  local copies, waits for them, and re-layouts  11.8 us (6%)
  other arithmetic  5.44 us (3%)
  matrix products  1.99 us (1%)
    all_gather x2, blocking collectives, collected_together(): both, at, found = (lax.all_gather(jnp.concatenate(lines), axis), 0, {})  50.6 us
    all_gather x2, blocking collectives, one_axis_at_a_time(): x = jnp.sum(lax.all_gather(x, axis), axis=0)  49.6 us
    all_to_all x3, blocking collectives, sent_to_all(): return lax.all_to_all(copies, axis, split_axis=0, concat_axis=0, tiled=True)  24.6 us
    all_to_all x1, starting transfers between devices, sent_to_all(): return lax.all_to_all(copies, axis, split_axis=0, concat_axis=0, tiled=True)  16.7 us
    all_to_all x1, waiting for transfers between devices, sum_by_axis(): return jnp.sum(lax.all_to_all(own, far, 0, 0, tiled=True), axis=0)  12 us
    all_to_all x1, waiting for transfers between devices, sent_to_all(): return lax.all_to_all(copies, axis, split_axis=0, concat_axis=0, tiled=True)  10.2 us
    unnamed x32, local copies, waits for them, and re-layouts  5 us
    all_to_all x1, starting transfers between devices, sum_by_axis(): return jnp.sum(lax.all_to_all(own, far, 0, 0, tiled=True), axis=0)  4.61 us
  transfers between devices with their start and end apart: 2, of which 2 were waited for; matrix products, arithmetic and copies ran while one was open for 1% of the time, Pallas kernels for 0%

profile of v1, /device:TPU:6, one launch (start us, length us, event | category | flops | bytes accessed | tf_op | source)
XLA Modules:
  0.0 191.9 jit_solution(4156310360947384974)
XLA Ops:
  0.0 1.4 broadcast_in_dim.8
  1.4 16.7 %all-to-all-start = ((bf16[64,4,32]{2,1,0:T(4,128)(2,1)}), bf16[64,4,32]{2,1,0:T(4,128)(2,1)S(1)}, u32[]{:S(2)}, u32[]{:S(2)}) async-start(bf16[64,4,32]{2,1,0:T(4,128)(2,1)} %broadcast_in_dim.8), calls=%async_computation | async-start | bytes 131072 | tf_op jit(solution)/shard_map/all_to_all | solution.py:15
  18.3 1.1 copy.24
  19.4 0.8 dynamic-slice
  20.1 10.2 %all-to-all-done = bf16[64,4,32]{2,1,0:T(4,128)(2,1)S(1)} async-done(((bf16[64,4,32]{2,1,0:T(4,128)(2,1)}), bf16[64,4,32]{2,1,0:T(4,128)(2,1)S(1)}, u32[]{:S(2)}, u32[]{:S(2)}) %all-to-all-start) | async-done | bytes 16416 | tf_op jit(solution)/shard_map/all_to_all | solution.py:15
  30.6 3.7 %all_to_all.30 = bf16[2,2,4096]{2,1,0:T(2,128)(2,1)S(1)} all-to-all(bf16[2,2,4096]{2,1,0:T(2,128)(2,1)S(1)} %reshape.2110), channel_id=1, replica_groups=mesh['dp'=4,'kv_0'=8,'kv_1'=8,'tp'=2] {'tp'}, dimensions={0} | all-to-all | bytes 65536 | tf_op jit(solution)/shard_map/all_to_all | solution.py:15
  34.9 0.7 copy-done.4
  35.6 0.2 convolution_bitcast_fusion.1
  35.8 24.8 %all-gather.4 = f32[8,4,2048]{2,1,0:T(4,128)S(1)} all-gather(f32[1,4,2048]{2,1,0:T(4,128)S(1)} %convolution_bitcast_fusion.1), channel_id=2, replica_groups=mesh['dp'=4,'kv_0'=8,'kv_1'=8,'tp'=2] {'kv_0'}, dimensions={0}, use_global_device_ids=true | all-gather | bytes 294912 | tf_op jit(solution)/shard_map/all_gather | solution.py:33
  60.6 24.8 %all-gather.5 = f32[8,4,2048]{2,1,0:T(4,128)S(1)} all-gather(f32[1,4,2048]{2,1,0:T(4,128)S(1)} %bitcast.440), channel_id=3, replica_groups=mesh['dp'=4,'kv_0'=8,'kv_1'=8,'tp'=2] {'kv_1'}, dimensions={0}, use_global_device_ids=true | all-gather | bytes 294912 | tf_op jit(solution)/shard_map/all_gather | solution.py:33
  85.8 0.3 fusion.98
  86.8 0.2 fusion.2
  87.1 25.3 %all-gather.6 = f32[8,130,128]{2,1,0:T(8,128)S(1)} all-gather(f32[1,130,128]{2,1,0:T(8,128)S(1)} %maximum_bitcast_fusion), channel_id=4, replica_groups=mesh['dp'=4,'kv_0'=8,'kv_1'=8,'tp'=2] {'kv_0'}, dimensions={0}, use_global_device_ids=true | all-gather | bytes 599040 | tf_op jit(solution)/shard_map/all_gather | solution.py:45
  112.5 0.3 fusion.9
  112.8 25.3 %all-gather.7 = f32[8,130,128]{2,1,0:T(8,128)S(1)} all-gather(f32[1,130,128]{2,1,0:T(8,128)S(1)} %maximum_bitcast_fusion.1), channel_id=5, replica_groups=mesh['dp'=4,'kv_0'=8,'kv_1'=8,'tp'=2] {'kv_1'}, dimensions={0}, use_global_device_ids=true | all-gather | bytes 599040 | tf_op jit(solution)/shard_map/all_gather | solution.py:45
  140.6 1.2 add_divide_fusion
  142.2 0.6 copy-done.5
  143.1 17.0 %all_to_all.31 = bf16[64,2,128]{2,1,0:T(2,128)(2,1)S(1)} all-to-all(bf16[64,2,128]{2,1,0:T(2,128)(2,1)S(1)} %reshape.2112), channel_id=1, replica_groups=mesh['dp'=4,'kv_0'=8,'kv_1'=8,'tp'=2] {'kv_0','kv_1'}, dimensions={0} | all-to-all | bytes 65536 | tf_op jit(solution)/shard_map/all_to_all | solution.py:15
  160.4 3.8 %all_to_all.32 = bf16[2,2,8192]{2,1,0:T(2,128)(2,1)S(1)} all-to-all(bf16[2,2,8192]{2,1,0:T(2,128)(2,1)S(1)} %reshape.2114), channel_id=1, replica_groups=mesh['dp'=4,'kv_0'=8,'kv_1'=8,'tp'=2] {'tp'}, dimensions={0} | all-to-all | bytes 131072 | tf_op jit(solution)/shard_map/all_to_all | solution.py:15
  164.4 0.4 bitcast_reduce_fusion
  165.2 0.7 copy-done.1
  165.9 0.3 fusion.94
  166.3 0.7 convolution_bitcast_fusion
  167.0 0.3 reshape_reshape.2
  167.5 3.8 %all_to_all.33 = f32[2,1,8192]{2,1,0:T(1,128)S(1)} all-to-all(f32[2,1,8192]{2,1,0:T(1,128)S(1)} %reshape.2116), channel_id=1, replica_groups=mesh['dp'=4,'kv_0'=8,'kv_1'=8,'tp'=2] {'tp'}, dimensions={0} | all-to-all | bytes 131072 | tf_op jit(solution)/shard_map/all_to_all | solution.py:71
  171.3 0.5 broadcast.374
  171.8 0.8 reduce.226
  172.9 0.7 reshape.2118
  173.7 4.6 %all-to-all-start.5 = ((f32[64,1,128]{2,1,0:T(1,128)}), f32[64,1,128]{2,1,0:T(1,128)S(1)}, u32[]{:S(2)}, u32[]{:S(2)}) async-start(f32[64,1,128]{2,1,0:T(1,128)} %reshape.2118), calls=%async_computation.5 | async-start | bytes 65536 | tf_op jit(solution)/shard_map/all_to_all | solution.py:78
  178.3 12.0 %all-to-all-done.5 = f32[64,1,128]{2,1,0:T(1,128)S(1)} async-done(((f32[64,1,128]{2,1,0:T(1,128)}), f32[64,1,128]{2,1,0:T(1,128)S(1)}, u32[]{:S(2)}, u32[]{:S(2)}) %all-to-all-start.5) | async-done | bytes 32800 | tf_op jit(solution)/shard_map/all_to_all | solution.py:78
  190.3 0.7 reduce.227
  191.3 0.6 fusion.44
  (89 shorter events, 6.7 us)
Async XLA Ops:
  0.0 166.3 %copy-start = (bf16[88,4096]{1,0:T(8,128)(2,1)S(1)}, bf16[88,4096]{1,0:T(8,128)(2,1)}, u32[]{:S(2)}) copy-start(bf16[88,4096]{1,0:T(8,128)(2,1)} %param.23) | copy-start | bytes 2162692
  1.4 16.7 %copy-start.7 = (f32[16]{0:T(128)S(1)}, f32[16]{0:T(128)}, u32[]{:S(2)}) copy-start(f32[16]{0:T(128)} %param.17) | copy-start | bytes 196
  1.4 16.7 %copy-start.8 = (f32[128]{0:T(128)S(1)}, f32[128]{0:T(128)}, u32[]{:S(2)}) copy-start(f32[128]{0:T(128)} %param.18) | copy-start | bytes 1540
  1.4 29.0 %all-to-all-start = ((bf16[64,4,32]{2,1,0:T(4,128)(2,1)}), bf16[64,4,32]{2,1,0:T(4,128)(2,1)S(1)}, u32[]{:S(2)}, u32[]{:S(2)}) async-start(bf16[64,4,32]{2,1,0:T(4,128)(2,1)} %broadcast_in_dim.8), calls=%async_computation | async-start | bytes 131072 | tf_op jit(solution)/shard_map/all_to_all | solution.py:15
  34.6 1.0 copy-start.4
  85.8 1.0 copy-start.3
  141.8 1.0 copy-start.5
  164.8 1.1 copy-start.1
  164.9 1.0 copy-start.6
  165.1 1.2 copy-start.2
  173.7 16.7 %all-to-all-start.5 = ((f32[64,1,128]{2,1,0:T(1,128)}), f32[64,1,128]{2,1,0:T(1,128)S(1)}, u32[]{:S(2)}, u32[]{:S(2)}) async-start(f32[64,1,128]{2,1,0:T(1,128)} %reshape.2118), calls=%async_computation.5 | async-start | bytes 65536 | tf_op jit(solution)/shard_map/all_to_all | solution.py:78
